TPU v7x, 128 devices: a whole 4x4x4 slice. The times are simulated.
128 devices in a mesh: kv: 16 (over z, x), tp: 8 (over y, core).
Axes of the slice: x: 4, y: 4, z: 4, core: 2. Of those that a mesh axis runs over, the one named last changes fastest.
Arguments:
- tokens: bfloat16 [32768, 2048], P('kv'), may hold values from -6 to 6
- norm_gain: bfloat16 [2048], replicated, may hold values from 0.099609375 to 1.8984375
- query_weight: bfloat16 [2048, 1024], P(None, 'tp'), may hold values from -0.125 to 0.125
- cmp_key_weight: bfloat16 [2048, 512], P(None, 'tp'), may hold values from -0.125 to 0.125
- cmp_value_weight: bfloat16 [2048, 512], P(None, 'tp'), may hold values from -0.125 to 0.125
- sel_key_weight: bfloat16 [2048, 512], P(None, 'tp'), may hold values from -0.125 to 0.125
- sel_value_weight: bfloat16 [2048, 512], P(None, 'tp'), may hold values from -0.125 to 0.125
- branch_weight: bfloat16 [2, 2048, 16], replicated, may hold values from -0.125 to 0.125
- key_embed: bfloat16 [8, 32, 64], P('tp'), may hold values from -3 to 3
- key_inner: bfloat16 [8, 2048, 64], P('tp'), may hold values from -0.125 to 0.125
- key_outer: bfloat16 [8, 64, 64], P('tp'), may hold values from -0.75 to 0.75
- value_embed: bfloat16 [8, 32, 64], P('tp'), may hold values from -3 to 3
- value_inner: bfloat16 [8, 2048, 64], P('tp'), may hold values from -0.125 to 0.125
- value_outer: bfloat16 [8, 64, 64], P('tp'), may hold values from -0.75 to 0.75
- out_weight: bfloat16 [1024, 2048], replicated, may hold values from -0.1875 to 0.1875
- chosen: int32 [8, 256, 8], P('tp'), may hold values from 0 to 511, as said below
Outputs:
- attended: bfloat16 [32768, 2048], P(('kv', 'tp'))
Inputs may be any that keep to these rules, and one draw needn't show every extreme that they name: `chosen`: each entry is the index of a block of 64 positions in the whole sequence. For every key head and query block, its 8 entries lie in 8 different aligned spans of 2048 positions (at most one from any span), and none lies inside the query block's own positions.
All inputs are finite; a program needn't handle non-finite values.
Results may differ from a plain program's by a relative error of at most 0.0075.
Values may be sent and summed in bfloat16 or wider, within the bound.
No kernel may reach another device: no remote copies, remote signals or barrier semaphores. Data moves between devices by JAX's collectives and lax.ppermute only.
A program may use at most 128 MiB of HBM per device.

v0:
```python
import jax
import jax.numpy as jnp
from jax import lax
from jax.sharding import PartitionSpec as P

HEAD_DIM = 64
CMP_BLOCK = 32
SEL_BLOCK = 64
Q_BLOCK = 128
FAR_PICKS = 8
ROPE_BASE = 10000.0
norm_eps = 1e-06
masked_score = -1000000000.0


def copy_for_each(x, axis):
    peers = lax.axis_size(axis)
    return lax.all_to_all(jnp.broadcast_to(x[None], (peers, *x.shape)), axis, 0, 0, tiled=True)


def in_order(pieces, dim):
    shape = list(pieces.shape[1:])
    shape[dim] *= pieces.shape[0]
    return jnp.moveaxis(pieces, 0, dim).reshape(shape)


def collect(x, axis, dim):
    pieces = copy_for_each(x, axis)
    return in_order(pieces, dim)


def rotate(values_in, positions):
    half_dim = values_in.shape[-1] // 2
    inverse = ROPE_BASE ** (-jnp.arange(half_dim, dtype=jnp.float32) / half_dim)
    rotary_phases = positions.astype(jnp.float32)[:, None] * inverse[None, :]
    cosine = jnp.cos(rotary_phases)[:, None, :]
    sine = jnp.sin(rotary_phases)[:, None, :]
    first_half = values_in[..., :half_dim]
    second_half = values_in[..., half_dim:]
    return jnp.concatenate(
        [first_half * cosine - second_half * sine, second_half * cosine + first_half * sine],
        axis=-1,
    )


def summarize(raw_rows, embed, inner, outer):
    kv_local = embed.shape[0]
    block_count = raw_rows.shape[0] // CMP_BLOCK
    blocked = (
        raw_rows.reshape(block_count, CMP_BLOCK, kv_local, HEAD_DIM)
        .transpose(2, 0, 1, 3)
        .astype(jnp.float32)
    )
    blocked = (blocked + embed.astype(jnp.float32)[:, None]).astype(jnp.bfloat16)
    blocked = blocked.reshape(kv_local, block_count, CMP_BLOCK * HEAD_DIM)
    hidden = jax.nn.gelu(
        jnp.einsum("knc,kce->kne", blocked, inner, preferred_element_type=jnp.float32)
    ).astype(jnp.bfloat16)
    return jnp.einsum("kne,kef->knf", hidden, outer, preferred_element_type=jnp.float32).astype(
        jnp.bfloat16
    )


def per_device(
    tokens,
    norm_gain,
    query_weight,
    cmp_key_weight,
    cmp_value_weight,
    sel_key_weight,
    sel_value_weight,
    branch_weight,
    key_embed,
    key_inner,
    key_outer,
    value_embed,
    value_inner,
    value_outer,
    out_weight,
    chosen,
):
    tok_rows = tokens.shape[0]
    kv_local = key_embed.shape[0]
    heads_local = query_weight.shape[1] // HEAD_DIM
    group_size = heads_local // kv_local
    owners = lax.axis_size("kv")
    dev_index = lax.axis_index("kv")
    offset = dev_index * tok_rows
    positions = offset + jnp.arange(tok_rows, dtype=jnp.int32)
    scale = HEAD_DIM ** (-0.5)
    expanded_mask = tokens.astype(jnp.float32)
    normed = (
        expanded_mask
        * lax.rsqrt(jnp.mean(expanded_mask * expanded_mask, axis=-1, keepdims=True) + norm_eps)
        * norm_gain.astype(jnp.float32)
    ).astype(jnp.bfloat16)
    gate_cols = lax.dynamic_slice_in_dim(
        branch_weight, lax.axis_index("tp") * heads_local, heads_local, 2
    )
    q_width = heads_local * HEAD_DIM
    kv_width = kv_local * HEAD_DIM
    joined_weight = jnp.concatenate(
        [
            query_weight,
            cmp_key_weight,
            cmp_value_weight,
            sel_key_weight,
            sel_value_weight,
            gate_cols[0],
            gate_cols[1],
        ],
        axis=1,
    )
    projected = jnp.dot(normed, joined_weight, preferred_element_type=jnp.float32)
    bounds = [
        q_width,
        q_width + kv_width,
        q_width + 2 * kv_width,
        q_width + 3 * kv_width,
        q_width + 4 * kv_width,
        q_width + 4 * kv_width + heads_local,
    ]
    (
        query_part,
        cmp_key_part,
        cmp_value_part,
        sel_key_part,
        sel_value_part,
        gate_cmp_part,
        gate_sel_part,
    ) = jnp.split(projected, bounds, axis=1)
    query = query_part.reshape(tok_rows, heads_local, HEAD_DIM)
    q_plain = query.astype(jnp.bfloat16)
    q_turn = rotate(query, positions).astype(jnp.bfloat16)
    cmp_key = cmp_key_part.astype(jnp.bfloat16).reshape(tok_rows, kv_local, HEAD_DIM)
    cmp_value = cmp_value_part.astype(jnp.bfloat16).reshape(tok_rows, kv_local, HEAD_DIM)
    sel_key = rotate(sel_key_part.reshape(tok_rows, kv_local, HEAD_DIM), positions).astype(
        jnp.bfloat16
    )
    selected_value = sel_value_part.astype(jnp.bfloat16).reshape(tok_rows, kv_local, HEAD_DIM)
    gate_cmp = jax.nn.sigmoid(gate_cmp_part)
    gate_sel = jax.nn.sigmoid(gate_sel_part)
    summary = jnp.concatenate(
        [
            summarize(cmp_key, key_embed, key_inner, key_outer),
            summarize(cmp_value, value_embed, value_inner, value_outer),
        ],
        axis=-1,
    )
    summaries = collect(summary, "kv", 1)
    summary_count = summaries.shape[1]
    block_end = (jnp.arange(summary_count, dtype=jnp.int32) + 1) * CMP_BLOCK - 1
    q_group = q_plain.reshape(tok_rows, kv_local, group_size, HEAD_DIM).transpose(1, 0, 2, 3)
    cmp_scores = (
        jnp.einsum(
            "ktgd,kcd->ktgc", q_group, summaries[..., :HEAD_DIM], preferred_element_type=jnp.float32
        )
        * scale
    )
    usable = (block_end[None, :] <= positions[:, None])[None, :, None, :]
    cmp_probs = jax.nn.softmax(
        jnp.where(usable, cmp_scores, masked_score), axis=-1
    ) * usable.astype(jnp.float32)
    out_cmp = jnp.einsum(
        "ktgc,kcd->ktgd",
        cmp_probs.astype(jnp.bfloat16),
        summaries[..., HEAD_DIM:],
        preferred_element_type=jnp.float32,
    )
    out_cmp = out_cmp.transpose(1, 0, 2, 3).reshape(tok_rows, heads_local, HEAD_DIM)
    span_queries = tok_rows // Q_BLOCK
    span_blocks = tok_rows // SEL_BLOCK
    kv_sel = jnp.concatenate([sel_key, selected_value], axis=-1).transpose(1, 0, 2)
    all_picks = chosen.reshape(kv_local, owners, span_queries, FAR_PICKS)
    my_picks = lax.dynamic_index_in_dim(all_picks, dev_index, 1, keepdims=False)
    head_lane = jnp.arange(kv_local, dtype=jnp.int32)[:, None, None]
    matches = all_picks // span_blocks == dev_index
    wanted = jnp.sum(jnp.where(matches, all_picks % span_blocks, 0), axis=3)
    blocked = kv_sel.reshape(kv_local, span_blocks, SEL_BLOCK, 2 * HEAD_DIM)
    outgoing = blocked[head_lane, wanted]
    incoming = lax.all_to_all(outgoing, "kv", split_axis=1, concat_axis=1, tiled=True)
    source = my_picks // span_blocks
    query_lane = jnp.arange(span_queries, dtype=jnp.int32)[None, :, None]
    picked = incoming[head_lane, source, query_lane]
    own_keys = kv_sel.reshape(kv_local, span_queries, Q_BLOCK, 2 * HEAD_DIM)
    keys_all = jnp.concatenate(
        [own_keys, picked.reshape(kv_local, span_queries, FAR_PICKS * SEL_BLOCK, 2 * HEAD_DIM)],
        axis=2,
    )
    query_pos = positions.reshape(span_queries, Q_BLOCK)
    far_pos = (my_picks[..., None] * SEL_BLOCK + jnp.arange(SEL_BLOCK, dtype=jnp.int32)).reshape(
        kv_local, span_queries, FAR_PICKS * SEL_BLOCK
    )
    key_pos = jnp.concatenate([query_pos[None], far_pos], axis=2)
    q_sel = q_turn.reshape(span_queries, Q_BLOCK, kv_local, group_size, HEAD_DIM).transpose(
        2, 0, 1, 3, 4
    )
    sel_scores = (
        jnp.einsum(
            "knqgd,knmd->knqgm", q_sel, keys_all[..., :HEAD_DIM], preferred_element_type=jnp.float32
        )
        * scale
    )
    allowed_keys = key_pos[:, :, None, None, :] <= query_pos[None, :, :, None, None]
    sel_probs = jax.nn.softmax(jnp.where(allowed_keys, sel_scores, masked_score), axis=-1)
    out_sel = jnp.einsum(
        "knqgm,knmd->knqgd",
        sel_probs.astype(jnp.bfloat16),
        keys_all[..., HEAD_DIM:],
        preferred_element_type=jnp.float32,
    )
    out_sel = out_sel.transpose(1, 2, 0, 3, 4).reshape(tok_rows, heads_local, HEAD_DIM)
    mixed = (
        (gate_cmp[..., None] * out_cmp + gate_sel[..., None] * out_sel)
        .reshape(tok_rows, heads_local * HEAD_DIM)
        .astype(jnp.bfloat16)
    )
    head_rows = lax.all_to_all(mixed, "tp", split_axis=0, concat_axis=1, tiled=True)
    return jnp.dot(head_rows, out_weight, preferred_element_type=jnp.float32).astype(jnp.bfloat16)


def solution(mesh):
    placed = (
        P("kv", None),
        P(),
        P(None, "tp"),
        P(None, "tp"),
        P(None, "tp"),
        P(None, "tp"),
        P(None, "tp"),
        P(),
        P("tp", None, None),
        P("tp", None, None),
        P("tp", None, None),
        P("tp", None, None),
        P("tp", None, None),
        P("tp", None, None),
        P(),
        P("tp", None, None),
    )
    return jax.shard_map(
        per_device, mesh=mesh, in_specs=placed, out_specs=P(("kv", "tp"), None), check_vma=False
    )
```

profile of v0, /device:TPU:1, one launch (start us, length us, event | category | flops | bytes accessed | tf_op | source)
XLA Modules:
  0.0 171.9 jit_solution(5051237416359795915)
XLA Ops:
  0.8 5.1 %fusion.2 = f32[2048]{0:T(1024)S(1)} fusion(bf16[2048,2048]{1,0:T(8,128)(2,1)} %param.16), kind=kLoop, calls=%fused_computation.6 | loop fusion | flops 12580864 | bytes 8396800 | tf_op jit(solution)/shard_map/reduce_sum | solution.py:94
  12.4 5.5 %concatenate.68 = bf16[2048,388]{1,0:T(8,128)(2,1)} concatenate(bf16[2048,128]{1,0:T(8,128)(2,1)} %param.18, bf16[2048,64]{1,0:T(8,128)(2,1)} %copy.58, bf16[2048,64]{1,0:T(8,128)(2,1)} %copy.59, bf16[2048,64]{1,0:T(8,128)(2,1)} %copy.60, bf16[2048,64]{1,0:T(8,128)(2,1)} %copy.61, bf16[2048,2]{1,0:T(8,128)(2,1)S(1)} %copy.62, bf16[2048,2]{1,0:T(8,128)(2,1)S(1)} %copy.63), dimensions={1} | concatenate | bytes 3178496 | tf_op jit(solution)/shard_map/concatenate | solution.py:102
  17.8 9.4 %fusion.119 = (bf16[2048,388]{0,1:T(8,128)(2,1)S(1)}, f32[2048,388]{0,1:T(8,128)}) fusion(bf16[2048,388]{1,0:T(8,128)(2,1)} %concatenate.68, bf16[2048,2048]{1,0:T(8,128)(2,1)} %param.16, f32[2048]{0:T(1024)S(1)} %convert_element_type.126, f32[2048]{0:T(1024)S(1)} %add_rsqrt_fusion), kind=kOutput, calls=%fused_computation.179 | convolution fusion | flops 3272351744 | bytes 14761984 | tf_op jit(solution)/shard_map/dot_general | solution.py:114
  27.4 1.0 copy-done.11
  31.5 8.5 %all-to-all-start = ((bf16[16,1,64,128]{3,2,1,0:T(8,128)(2,1)}), bf16[16,1,64,128]{3,2,1,0:T(8,128)(2,1)}, u32[]{:S(2)}, u32[]{:S(2)}) async-start(bf16[16,1,64,128]{3,2,1,0:T(8,128)(2,1)} %broadcast_in_dim.34), calls=%async_computation | async-start | bytes 524288 | tf_op jit(solution)/shard_map/all_to_all | solution.py:18
  40.2 1.7 %slice_bitcast_fusion.14 = (bf16[8,8,16,128]{3,1,2,0:T(8,128)(2,1)}, bf16[2048,64]{0,1:T(8,128)(2,1)S(1)}) fusion(bf16[2048,388]{0,1:T(8,128)(2,1)} %copy-done.11), kind=kLoop, calls=%fused_computation.176 | loop fusion | bytes 786432
  41.9 1.6 fusion.78
  43.5 1.1 slice_bitcast_fusion.4
  44.5 1.3 split.34
  46.7 1.8 %multiply_cosine_fusion.1 = (f32[2048,32]{0,1:T(8,128)}, f32[2048,32]{0,1:T(8,128)}) fusion(f32[32]{0:T(128)S(1)} %multiply_power_fusion, f32[2048]{0:T(1024)S(1)} %get-tuple-element.30), kind=kLoop, calls=%fused_computation.56 | loop fusion | flops 65536 | bytes 532608 | tf_op jit(solution)/shard_map/cos | solution.py:36
  48.5 1.1 fusion.35
  50.3 1.8 %broadcast_compare_fusion.1 = pred[16,128,640]{2,1,0:T(8,128)(4,1)} fusion(s32[16,128]{1,0:T(8,128)S(1)} %add_add_fusion, s32[16,640]{1,0:T(8,128)S(1)} %add_bitcast_fusion), kind=kLoop, calls=%fused_computation.30 | loop fusion | flops 1310720 | bytes 1359872 | tf_op jit(solution)/shard_map/le | solution.py:204
  52.5 3.1 %gather_fusion = bf16[256,64,128]{2,1,0:T(8,128)(2,1)} fusion(bf16[1,32,64,128]{3,2,1,0:T(8,128)(2,1)S(1)} %pad_maximum_fusion.1, s32[256]{0:T(256)S(1)} %reshape.731), kind=kCustom, calls=%fused_computation | custom fusion | bytes 8390656 | tf_op jit(solution)/shard_map/gather | solution.py:180
  55.8 6.8 %all-to-all-start.1 = ((bf16[1,16,16,64,128]{4,3,2,0,1:T(8,128)(2,1)}), bf16[1,16,16,64,128]{4,3,2,0,1:T(8,128)(2,1)}, u32[]{:S(2)}, u32[]{:S(2)}) async-start(bf16[1,16,16,64,128]{4,3,2,0,1:T(8,128)(2,1)} %bitcast.158), calls=%async_computation.1 | async-start | bytes 8388608 | tf_op jit(solution)/shard_map/all_to_all | solution.py:181
  62.6 2.1 %split.57 = bf16[2048,128]{0,1:T(8,128)(2,1)} slice(f32[2048,388]{0,1:T(8,128)} %get-tuple-element.24), slice={[0:2048], [0:128]} | slice | bytes 1048576 | tf_op jit(solution)/shard_map/split | solution.py:131
  68.5 4.2 %fusion.118 = (f32[2048,1024]{0,1:T(8,128)}, pred[2048,1024]{0,1:T(8,128)(4,1)S(1)}) fusion(s32[2048]{0:T(1024)S(1)} %get-tuple-element.29, s32[1024]{0:T(1024)S(1)} %multiply_add_fusion), kind=kLoop, calls=%fused_computation.178 | loop fusion | flops 4194304 | bytes 10498048 | tf_op jit(solution)/shard_map/convert_element_type | solution.py:163
  72.6 10.6 %fusion.121 = (f32[2048,2]{0,1:T(2,128)S(1)}, f32[2048,2,1024]{0,2,1:T(8,128)}) fusion(pred[2048,1024]{0,1:T(8,128)(4,1)S(1)} %get-tuple-element.20, bf16[2048,2,64]{0,2,1:T(8,128)(2,1)} %bitcast.173, bf16[1,1024,128]{2,1,0:T(8,128)(2,1)} %bitcast.14), kind=kOutput, calls=%fused_computation.181 | convolution fusion | flops 553649152 | bytes 19677184 | tf_op jit(solution)/shard_map/sub | solution.py:161
  83.3 9.4 %fusion.19 = f32[2048,2,64]{0,2,1:T(8,128)S(1)} fusion(f32[2048,2,1024]{0,2,1:T(8,128)} %get-tuple-element.28, f32[2048,1024]{0,1:T(8,128)} %get-tuple-element.19, f32[2048,2]{0,1:T(2,128)S(1)} %get-tuple-element.27, f32[2048,2]{0,1:T(2,128)S(1)} %copy-done.20, bf16[1,1024,128]{2,1,0:T(8,128)(2,1)} %bitcast.14), kind=kOutput, calls=%fused_computation.32 | convolution fusion | flops 549715968 | bytes 26509312 | tf_op jit(solution)/shard_map/ktgc,kcd->ktgd/dot_general | solution.py:164
  92.7 1.3 copy.96
  94.0 29.5 %all-to-all-done.1 = bf16[1,16,16,64,128]{4,3,2,0,1:T(8,128)(2,1)} async-done(((bf16[1,16,16,64,128]{4,3,2,0,1:T(8,128)(2,1)}), bf16[1,16,16,64,128]{4,3,2,0,1:T(8,128)(2,1)}, u32[]{:S(2)}, u32[]{:S(2)}) %all-to-all-start.1) | async-done | bytes 4194336 | tf_op jit(solution)/shard_map/all_to_all | solution.py:181
  123.5 4.5 %gather_fusion.1 = bf16[128,64,128]{2,1,0:T(8,128)(2,1)} fusion(bf16[1,16,16,64,128]{4,3,2,1,0:T(8,128)(2,1)} %bitcast.29, s32[128]{0:T(128)S(1)} %reshape.739), kind=kCustom, calls=%fused_computation.1 | custom fusion | bytes 4195840 | tf_op jit(solution)/shard_map/gather | solution.py:184
  127.9 2.9 %copy.83 = bf16[1,16,512,128]{2,3,1,0:T(8,128)(2,1)S(1)} copy(bf16[1,16,512,128]{3,2,1,0:T(8,128)(2,1)} %bitcast.159) | data formatting | bytes 4194304 | tf_op jit(solution)/shard_map/reshape | solution.py:187
  130.9 1.3 pad_maximum_fusion
  132.2 1.6 copy-done.2
  133.8 1.6 fusion.22
  135.4 7.2 %fusion.120 = (f32[16,128,2]{1,2,0:T(2,128)S(1)}, f32[16,128,2,640]{3,1,2,0:T(8,128)}) fusion(f32[16,128,2,640]{3,1,2,0:T(8,128)S(1)} %fusion.22, pred[16,128,640]{2,1,0:T(8,128)(4,1)S(1)} %copy-done.5), kind=kOutput, calls=%fused_computation.180 | output fusion | flops 15729279 | bytes 22298624 | tf_op jit(solution)/shard_map/sub | solution.py:205
  142.5 5.4 %fusion.18 = f32[16,128,2,64]{1,3,2,0:T(8,128)S(1)} fusion(f32[16,128,2,640]{3,1,2,0:T(8,128)} %get-tuple-element.26, f32[16,128,2]{1,2,0:T(2,128)S(1)} %get-tuple-element.25, bf16[1,16,640,128]{2,3,1,0:T(8,128)(2,1)S(1)} %copy-done.3), kind=kOutput, calls=%fused_computation.27 | convolution fusion | flops 340787200 | bytes 12861440 | tf_op jit(solution)/shard_map/knqgm,knmd->knqgd/dot_general | solution.py:206
  148.0 1.6 copy.84
  149.5 2.5 %reshape_transpose.10 = f32[8,256,128]{1,0,2:T(8,128)} reshape(f32[16,128,2,64]{1,0,3,2:T(8,128)} %copy.84) | data formatting | bytes 2097152 | tf_op jit(solution)/shard_map/reshape;transpose | solution.py:212
  152.1 1.6 fusion.26
  153.7 15.9 %all_to_all.26 = bf16[8,256,128]{1,2,0:T(8,128)(2,1)S(1)} all-to-all(bf16[8,256,128]{1,2,0:T(8,128)(2,1)S(1)} %copy.85), channel_id=1, replica_groups=mesh['kv'=16,'tp'=8] {'tp'}, dimensions={0} | all-to-all | bytes 1048576 | tf_op jit(solution)/shard_map/all_to_all | solution.py:218
  169.6 2.2 %convolution_convert_fusion = bf16[256,2048]{1,0:T(8,128)(2,1)} fusion(bf16[256,1024]{0,1:T(8,128)(2,1)S(1)} %bitcast.174, bf16[1024,2048]{1,0:T(8,128)(2,1)S(1)} %copy-done.23), kind=kOutput, calls=%fused_computation.31 | convolution fusion | flops 1074266112 | bytes 5767168 | tf_op jit(solution)/shard_map/dot_general | solution.py:219
  (114 shorter events, 16.4 us)
Async XLA Ops:
  0.0 29.9 %copy-start = (bf16[1,2048,64]{1,2,0:T(8,128)(2,1)S(1)}, bf16[1,2048,64]{1,2,0:T(8,128)(2,1)}, u32[]{:S(2)}) copy-start(bf16[1,2048,64]{1,2,0:T(8,128)(2,1)} %param.25) | copy-start | bytes 786436
  0.0 5.9 %copy-start.21 = (bf16[1,32,64]{2,1,0:T(8,128)(2,1)S(1)}, bf16[1,32,64]{2,1,0:T(8,128)(2,1)}, u32[]{:S(2)}) copy-start(bf16[1,32,64]{2,1,0:T(8,128)(2,1)} %param.24) | copy-start | bytes 12292
  0.0 6.0 %copy-start.22 = (bf16[1,32,64]{2,1,0:T(8,128)(2,1)S(1)}, bf16[1,32,64]{2,1,0:T(8,128)(2,1)}, u32[]{:S(2)}) copy-start(bf16[1,32,64]{2,1,0:T(8,128)(2,1)} %param.27) | copy-start | bytes 12292
  0.0 7.4 %copy-start.12 = (bf16[2048,64]{0,1:T(8,128)(2,1)S(1)}, bf16[2048,64]{0,1:T(8,128)(2,1)}, u32[]{:S(2)}) copy-start(bf16[2048,64]{0,1:T(8,128)(2,1)} %param.19) | copy-start | bytes 786436
  0.0 8.4 %copy-start.13 = (bf16[2048,64]{0,1:T(8,128)(2,1)S(1)}, bf16[2048,64]{0,1:T(8,128)(2,1)}, u32[]{:S(2)}) copy-start(bf16[2048,64]{0,1:T(8,128)(2,1)} %param.20) | copy-start | bytes 786436
  0.8 8.7 %copy-start.14 = (bf16[2048,64]{0,1:T(8,128)(2,1)S(1)}, bf16[2048,64]{0,1:T(8,128)(2,1)}, u32[]{:S(2)}) copy-start(bf16[2048,64]{0,1:T(8,128)(2,1)} %param.21) | copy-start | bytes 786436
  0.8 9.7 %copy-start.15 = (bf16[2048,64]{0,1:T(8,128)(2,1)S(1)}, bf16[2048,64]{0,1:T(8,128)(2,1)}, u32[]{:S(2)}) copy-start(bf16[2048,64]{0,1:T(8,128)(2,1)} %param.22) | copy-start | bytes 786436
  27.2 1.2 copy-start.11
  27.2 2.7 %copy-start.18 = (bf16[1,64,64]{2,1,0:T(8,128)(2,1)S(1)}, bf16[1,64,64]{2,1,0:T(8,128)(2,1)}, u32[]{:S(2)}) copy-start(bf16[1,64,64]{2,1,0:T(8,128)(2,1)} %param.26) | copy-start | bytes 24580
  27.2 3.0 %copy-start.16 = (bf16[1,2048,64]{1,2,0:T(8,128)(2,1)S(1)}, bf16[1,2048,64]{1,2,0:T(8,128)(2,1)}, u32[]{:S(2)}) copy-start(bf16[1,2048,64]{1,2,0:T(8,128)(2,1)} %param.28) | copy-start | bytes 786436
  27.2 3.1 %copy-start.19 = (bf16[1,64,64]{2,1,0:T(8,128)(2,1)S(1)}, bf16[1,64,64]{2,1,0:T(8,128)(2,1)}, u32[]{:S(2)}) copy-start(bf16[1,64,64]{2,1,0:T(8,128)(2,1)} %param.29) | copy-start | bytes 24580
  27.2 12.8 %copy-start.17 = (s32[1,256,8]{1,2,0:T(8,128)S(1)}, s32[1,256,8]{1,2,0:T(8,128)}, u32[]{:S(2)}) copy-start(s32[1,256,8]{1,2,0:T(8,128)} %param.31) | copy-start | bytes 24580
  31.5 24.3 %all-to-all-start = ((bf16[16,1,64,128]{3,2,1,0:T(8,128)(2,1)}), bf16[16,1,64,128]{3,2,1,0:T(8,128)(2,1)}, u32[]{:S(2)}, u32[]{:S(2)}) async-start(bf16[16,1,64,128]{3,2,1,0:T(8,128)(2,1)} %broadcast_in_dim.34), calls=%async_computation | async-start | bytes 524288 | tf_op jit(solution)/shard_map/all_to_all | solution.py:18
  52.5 3.1 %copy-start.9 = (f32[2048,32]{0,1:T(8,128)S(1)}, f32[2048,32]{0,1:T(8,128)}, u32[]{:S(2)}) copy-start(f32[2048,32]{0,1:T(8,128)} %get-tuple-element.21) | copy-start | bytes 786436
  52.5 3.1 %copy-start.10 = (f32[2048,32]{0,1:T(8,128)S(1)}, f32[2048,32]{0,1:T(8,128)}, u32[]{:S(2)}) copy-start(f32[2048,32]{0,1:T(8,128)} %get-tuple-element.22) | copy-start | bytes 786436
  55.8 9.1 %copy-start.6 = (bf16[8,8,16,128]{3,1,2,0:T(8,128)(2,1)S(1)}, bf16[8,8,16,128]{3,1,2,0:T(8,128)(2,1)}, u32[]{:S(2)}) copy-start(bf16[8,8,16,128]{3,1,2,0:T(8,128)(2,1)} %get-tuple-element.11) | copy-start | bytes 786436
  55.8 67.7 %all-to-all-start.1 = ((bf16[1,16,16,64,128]{4,3,2,0,1:T(8,128)(2,1)}), bf16[1,16,16,64,128]{4,3,2,0,1:T(8,128)(2,1)}, u32[]{:S(2)}, u32[]{:S(2)}) async-start(bf16[1,16,16,64,128]{4,3,2,0,1:T(8,128)(2,1)} %bitcast.158), calls=%async_computation.1 | async-start | bytes 8388608 | tf_op jit(solution)/shard_map/all_to_all | solution.py:181
  72.6 10.6 %copy-start.20 = (f32[2048,2]{0,1:T(2,128)S(1)}, f32[2048,2]{0,1:T(2,128)}, u32[]{:S(2)}) copy-start(f32[2048,2]{0,1:T(2,128)} %get-tuple-element.7) | copy-start | bytes 49156
  127.9 5.8 %copy-start.7 = (bf16[2,4,16,8,128]{4,3,1,0,2:T(8,128)(2,1)S(1)}, bf16[2,4,16,8,128]{4,3,1,0,2:T(8,128)(2,1)}, u32[]{:S(2)}) copy-start(bf16[2,4,16,8,128]{4,3,1,0,2:T(8,128)(2,1)} %copy.104) | copy-start | bytes 786436
  130.8 2.9 %copy-start.8 = (bf16[2,4,16,8,128]{4,3,1,0,2:T(8,128)(2,1)S(1)}, bf16[2,4,16,8,128]{4,3,1,0,2:T(8,128)(2,1)}, u32[]{:S(2)}) copy-start(bf16[2,4,16,8,128]{4,3,1,0,2:T(8,128)(2,1)} %copy.103) | copy-start | bytes 786436
  132.2 1.6 copy-start.2
  133.8 1.6 copy-start.5
  135.3 7.2 %copy-start.3 = (bf16[1,16,640,128]{2,3,1,0:T(8,128)(2,1)S(1)}, bf16[1,16,640,128]{2,3,1,0:T(8,128)(2,1)}, u32[]{:S(2)}) copy-start(bf16[1,16,640,128]{2,3,1,0:T(8,128)(2,1)} %copy-done.2) | copy-start | bytes 7864324
  142.5 9.5 %copy-start.4 = (f32[16,8,8,256]{3,2,1,0:T(8,128)S(1)}, f32[16,8,8,256]{3,2,1,0:T(8,128)}, u32[]{:S(2)}) copy-start(f32[16,8,8,256]{3,2,1,0:T(8,128)} %copy.96) | copy-start | bytes 3145732
  152.1 17.6 %copy-start.23 = (bf16[1024,2048]{1,0:T(8,128)(2,1)S(1)}, bf16[1024,2048]{1,0:T(8,128)(2,1)}, u32[]{:S(2)}) copy-start(bf16[1024,2048]{1,0:T(8,128)(2,1)} %param.30) | copy-start | bytes 12582916
  152.1 19.8 %copy-start.1 = (bf16[1,2048,64]{1,2,0:T(8,128)(2,1)S(1)}, bf16[1,2048,64]{1,2,0:T(8,128)(2,1)}, u32[]{:S(2)}) copy-start(bf16[1,2048,64]{1,2,0:T(8,128)(2,1)} %param.25) | copy-start | bytes 786436
where the time goes:
time: 173 us; the launch traced here: 172 us
  local copies, waits for them, and re-layouts  44 us (25%)
  matrix products  39.3 us (23%)
  waiting for transfers between devices  29.5 us (17%)
  other arithmetic  27.4 us (16%)
  blocking collectives  15.9 us (9%)
  starting transfers between devices  15.3 us (9%)
    all_to_all x1, waiting for transfers between devices, per_device(): lax.all_to_all(outgoing, 'kv', split_axis=1, concat_axis=1, tiled=True)  29.5 us
    all_to_all x1, blocking collectives, per_device(): lax.all_to_all(mixed, 'tp', split_axis=0, concat_axis=1, tiled=True)  15.9 us
    sub x1, matrix products, per_device(): jax.nn.softmax(jnp.where(usable, cmp_scores, masked_score), axis=-1)  10.6 us
    unnamed x58, local copies, waits for them, and re-layouts  10.2 us
    dot_general x1, matrix products, per_device(): jnp.einsum('ktgc,kcd->ktgd', cmp_probs.astype(jnp.bfloat16), summaries[.....  9.4 us
    dot_general x1, matrix products, per_device(): jnp.dot(normed, joined_weight, preferred_element_type=jnp.float32)  9.36 us
    all_to_all x1, starting transfers between devices, copy_for_each(): lax.all_to_all(jnp.broadcast_to(x[None], (peers, *x.shape)), axis, 0, 0,...  8.48 us
    sub x1, other arithmetic, per_device(): jax.nn.softmax(jnp.where(allowed_keys, sel_scores, masked_score), axis=-1)  7.17 us
  transfers between devices with their start and end apart: 2, of which 1 were waited for; matrix products, arithmetic and copies ran while one was open for 27% of the time, Pallas kernels for 0%

commit v1 on v0

--- a/solution.py
+++ b/solution.py
@@ -215,7 +215,9 @@
         .reshape(tok_rows, heads_local * HEAD_DIM)
         .astype(jnp.bfloat16)
     )
-    head_rows = lax.all_to_all(mixed, "tp", split_axis=0, concat_axis=1, tiled=True)
+    head_rows = jnp.concatenate(
+        lax.all_to_all(jnp.stack(jnp.split(mixed, lax.axis_size("tp"), axis=0)), "tp", 0, 0), axis=1
+    )
     return jnp.dot(head_rows, out_weight, preferred_element_type=jnp.float32).astype(jnp.bfloat16)
 
 

time: 173 us -> 167 us (0.965)
  local copies, waits for them, and re-layouts: 44 us -> 35.9 us
  other arithmetic: 27.4 us -> 24.6 us
  waiting for transfers between devices: 29.5 us -> 32.1 us
  matrix products: 39.3 us -> 41.1 us
    all_to_all x1, waiting for transfers between devices: 29.5 us -> 32.1 us  [per_device(): lax.all_to_all(outgoing, 'kv', split_axis=1, concat_axis=1, tiled=True)]
    another operation x1, local copies, waits for them, and re-layouts: 2.51 us -> 0.01 us  [per_device(): jnp.stack(jnp.split(mixed, lax.axis_size('tp'), axis=0))]
    concatenate x6, local copies, waits for them, and re-layouts: 2.81 us -> 0.74 us  [rotate(): jnp.concatenate([first_half * cosine - second_half * sine, second_half *...]
    dot_general x1, matrix products: 9.4 us -> 11.3 us  [per_device(): jnp.einsum('ktgc,kcd->ktgd', cmp_probs.astype(jnp.bfloat16), summaries[.....]
    unnamed x58 -> x57, local copies, waits for them, and re-layouts: 10.2 us -> 8.6 us
  transfers between devices with their start and end apart: 2 -> 2, of which waited for: 1 -> 1; matrix products, arithmetic and copies ran while one was open for 27% -> 26% of each run, Pallas kernels for 0% -> 0%
where the time goes in v1:
time: 167 us; the launch traced here: 166 us
  matrix products  41.1 us (25%)
  local copies, waits for them, and re-layouts  35.9 us (21%)
  waiting for transfers between devices  32.1 us (19%)
  other arithmetic  24.6 us (15%)
  blocking collectives  16 us (10%)
  starting transfers between devices  15.3 us (9%)
    all_to_all x1, waiting for transfers between devices, per_device(): lax.all_to_all(outgoing, 'kv', split_axis=1, concat_axis=1, tiled=True)  32.1 us
    all_to_all x1, blocking collectives, per_device(): lax.all_to_all(jnp.stack(jnp.split(mixed, lax.axis_size('tp'), axis=0)),...  16 us
    dot_general x1, matrix products, per_device(): jnp.einsum('ktgc,kcd->ktgd', cmp_probs.astype(jnp.bfloat16), summaries[.....  11.3 us
    sub x1, matrix products, per_device(): jax.nn.softmax(jnp.where(usable, cmp_scores, masked_score), axis=-1)  10.7 us
    dot_general x1, matrix products, per_device(): jnp.dot(normed, joined_weight, preferred_element_type=jnp.float32)  9.37 us
    unnamed x57, local copies, waits for them, and re-layouts  8.6 us
    all_to_all x1, starting transfers between devices, copy_for_each(): lax.all_to_all(jnp.broadcast_to(x[None], (peers, *x.shape)), axis, 0, 0,...  8.48 us
    sub x1, other arithmetic, per_device(): jax.nn.softmax(jnp.where(allowed_keys, sel_scores, masked_score), axis=-1)  7.14 us
  transfers between devices with their start and end apart: 2, of which 1 were waited for; matrix products, arithmetic and copies ran while one was open for 26% of the time, Pallas kernels for 0%

profile of v1, /device:TPU:1, one launch (start us, length us, event | category | flops | bytes accessed | tf_op | source)
XLA Modules:
  0.0 165.6 jit_solution(8321500910990705629)
XLA Ops:
  0.8 5.1 %fusion.2 = f32[2048]{0:T(1024)S(1)} fusion(bf16[2048,2048]{1,0:T(8,128)(2,1)} %param.16), kind=kLoop, calls=%fused_computation.6 | loop fusion | flops 12580864 | bytes 8396800 | tf_op jit(solution)/shard_map/reduce_sum | solution.py:94
  6.0 0.8 dynamic-slice_bitcast_fusion
  7.4 1.0 copy.57
  8.4 1.0 copy.58
  9.5 1.0 copy.59
  10.5 1.0 copy.60
  12.4 5.5 %concatenate.68 = bf16[2048,388]{1,0:T(8,128)(2,1)} concatenate(bf16[2048,128]{1,0:T(8,128)(2,1)} %param.18, bf16[2048,64]{1,0:T(8,128)(2,1)} %copy.57, bf16[2048,64]{1,0:T(8,128)(2,1)} %copy.58, bf16[2048,64]{1,0:T(8,128)(2,1)} %copy.59, bf16[2048,64]{1,0:T(8,128)(2,1)} %copy.60, bf16[2048,2]{1,0:T(8,128)(2,1)S(1)} %copy.61, bf16[2048,2]{1,0:T(8,128)(2,1)S(1)} %copy.62), dimensions={1} | concatenate | bytes 3178496 | tf_op jit(solution)/shard_map/concatenate | solution.py:102
  17.9 9.4 %fusion.127 = (bf16[2048,388]{0,1:T(8,128)(2,1)S(1)}, f32[2048,388]{0,1:T(8,128)}) fusion(bf16[2048,388]{1,0:T(8,128)(2,1)} %concatenate.68, bf16[2048,2048]{1,0:T(8,128)(2,1)} %param.16, f32[2048]{0:T(1024)S(1)} %convert_element_type.125, f32[2048]{0:T(1024)S(1)} %add_rsqrt_fusion), kind=kOutput, calls=%fused_computation.195 | convolution fusion | flops 3272351744 | bytes 14761984 | tf_op jit(solution)/shard_map/dot_general | solution.py:114
  27.4 1.0 copy-done.9
  31.5 8.5 %all-to-all-start = ((bf16[16,1,64,128]{3,2,1,0:T(8,128)(2,1)}), bf16[16,1,64,128]{3,2,1,0:T(8,128)(2,1)}, u32[]{:S(2)}, u32[]{:S(2)}) async-start(bf16[16,1,64,128]{3,2,1,0:T(8,128)(2,1)} %broadcast_in_dim.34), calls=%async_computation | async-start | bytes 524288 | tf_op jit(solution)/shard_map/all_to_all | solution.py:18
  40.2 1.7 %slice_bitcast_fusion.22 = (bf16[8,8,16,128]{3,1,2,0:T(8,128)(2,1)}, bf16[2048,64]{0,1:T(8,128)(2,1)S(1)}) fusion(bf16[2048,388]{0,1:T(8,128)(2,1)} %copy-done.9), kind=kLoop, calls=%fused_computation.192 | loop fusion | bytes 786432
  41.9 1.0 fusion.83
  42.9 1.1 slice_bitcast_fusion.4
  44.0 1.3 split.66
  46.1 1.8 %multiply_cosine_fusion.1 = (f32[2048,32]{0,1:T(8,128)}, f32[2048,32]{0,1:T(8,128)}) fusion(f32[32]{0:T(128)S(1)} %multiply_power_fusion, f32[2048]{0:T(1024)S(1)} %get-tuple-element.30), kind=kLoop, calls=%fused_computation.56 | loop fusion | flops 65536 | bytes 532608 | tf_op jit(solution)/shard_map/cos | solution.py:36
  48.0 1.1 fusion.35
  49.7 1.7 %broadcast_compare_fusion.1 = pred[16,128,640]{2,1,0:T(8,128)(4,1)} fusion(s32[16,128]{1,0:T(8,128)S(1)} %add_add_fusion, s32[16,640]{1,0:T(8,128)S(1)} %add_bitcast_fusion), kind=kLoop, calls=%fused_computation.30 | loop fusion | flops 1310720 | bytes 1359872 | tf_op jit(solution)/shard_map/le | solution.py:204
  51.9 3.1 %gather_fusion = bf16[256,64,128]{2,1,0:T(8,128)(2,1)} fusion(bf16[1,32,64,128]{3,2,1,0:T(8,128)(2,1)S(1)} %pad_maximum_fusion.1, s32[256]{0:T(256)S(1)} %reshape.732), kind=kCustom, calls=%fused_computation | custom fusion | bytes 8390656 | tf_op jit(solution)/shard_map/gather | solution.py:180
  55.2 6.8 %all-to-all-start.1 = ((bf16[1,16,16,64,128]{4,3,2,0,1:T(8,128)(2,1)}), bf16[1,16,16,64,128]{4,3,2,0,1:T(8,128)(2,1)}, u32[]{:S(2)}, u32[]{:S(2)}) async-start(bf16[1,16,16,64,128]{4,3,2,0,1:T(8,128)(2,1)} %bitcast.184), calls=%async_computation.1 | async-start | bytes 8388608 | tf_op jit(solution)/shard_map/all_to_all | solution.py:181
  62.0 2.1 %split.121 = bf16[2048,128]{0,1:T(8,128)(2,1)} slice(f32[2048,388]{0,1:T(8,128)} %get-tuple-element.24), slice={[0:2048], [0:128]} | slice | bytes 1048576 | tf_op jit(solution)/shard_map/split | solution.py:131
  64.7 4.2 %fusion.126 = (f32[2048,1024]{0,1:T(8,128)}, pred[2048,1024]{0,1:T(8,128)(4,1)S(1)}) fusion(s32[2048]{0:T(1024)S(1)} %get-tuple-element.29, s32[1024]{0:T(1024)S(1)} %multiply_add_fusion), kind=kLoop, calls=%fused_computation.194 | loop fusion | flops 4194304 | bytes 10498048 | tf_op jit(solution)/shard_map/convert_element_type | solution.py:163
  68.8 10.7 %fusion.129 = (f32[2048,2]{0,1:T(2,128)S(1)}, f32[2048,2,1024]{0,2,1:T(8,128)}) fusion(pred[2048,1024]{0,1:T(8,128)(4,1)S(1)} %get-tuple-element.20, bf16[2048,2,64]{0,2,1:T(8,128)(2,1)} %bitcast.198, bf16[1,1024,128]{2,1,0:T(8,128)(2,1)} %bitcast.14), kind=kOutput, calls=%fused_computation.197 | convolution fusion | flops 553649152 | bytes 19677184 | tf_op jit(solution)/shard_map/sub | solution.py:161
  79.5 11.3 %fusion.19 = f32[2048,2,64]{0,2,1:T(8,128)} fusion(f32[2048,2,1024]{0,2,1:T(8,128)} %get-tuple-element.28, f32[2048,1024]{0,1:T(8,128)} %get-tuple-element.19, f32[2048,2]{0,1:T(2,128)S(1)} %get-tuple-element.27, f32[2048,2]{0,1:T(2,128)S(1)} %get-tuple-element.8, bf16[1,1024,128]{2,1,0:T(8,128)(2,1)} %bitcast.14), kind=kOutput, calls=%fused_computation.32 | convolution fusion | flops 549715968 | bytes 26509312 | tf_op jit(solution)/shard_map/ktgc,kcd->ktgd/dot_general | solution.py:164
  90.8 32.1 %all-to-all-done.1 = bf16[1,16,16,64,128]{4,3,2,0,1:T(8,128)(2,1)} async-done(((bf16[1,16,16,64,128]{4,3,2,0,1:T(8,128)(2,1)}), bf16[1,16,16,64,128]{4,3,2,0,1:T(8,128)(2,1)}, u32[]{:S(2)}, u32[]{:S(2)}) %all-to-all-start.1) | async-done | bytes 4194336 | tf_op jit(solution)/shard_map/all_to_all | solution.py:181
  122.9 4.5 %gather_fusion.1 = bf16[128,64,128]{2,1,0:T(8,128)(2,1)} fusion(bf16[1,16,16,64,128]{4,3,2,1,0:T(8,128)(2,1)} %bitcast.31, s32[128]{0:T(128)S(1)} %reshape.740), kind=kCustom, calls=%fused_computation.1 | custom fusion | bytes 4195840 | tf_op jit(solution)/shard_map/gather | solution.py:184
  127.3 2.9 %copy.82 = bf16[1,16,512,128]{2,3,1,0:T(8,128)(2,1)S(1)} copy(bf16[1,16,512,128]{3,2,1,0:T(8,128)(2,1)} %bitcast.185) | data formatting | bytes 4194304 | tf_op jit(solution)/shard_map/reshape | solution.py:187
  130.6 1.6 copy-done.2
  132.1 1.6 fusion.22
  133.7 7.1 %fusion.128 = (f32[16,128,2]{1,2,0:T(2,128)S(1)}, f32[16,128,2,640]{3,1,2,0:T(8,128)}) fusion(f32[16,128,2,640]{3,1,2,0:T(8,128)S(1)} %fusion.22, pred[16,128,640]{2,1,0:T(8,128)(4,1)S(1)} %copy-done.4), kind=kOutput, calls=%fused_computation.196 | output fusion | flops 15729279 | bytes 22298624 | tf_op jit(solution)/shard_map/sub | solution.py:205
  140.9 5.2 %fusion.18 = f32[16,128,2,64]{1,3,2,0:T(8,128)S(1)} fusion(f32[16,128,2,640]{3,1,2,0:T(8,128)} %get-tuple-element.26, f32[16,128,2]{1,2,0:T(2,128)S(1)} %get-tuple-element.25, bf16[1,16,640,128]{2,3,1,0:T(8,128)(2,1)S(1)} %copy-done.3), kind=kOutput, calls=%fused_computation.27 | convolution fusion | flops 340787200 | bytes 12861440 | tf_op jit(solution)/shard_map/knqgm,knmd->knqgd/dot_general | solution.py:206
  147.3 16.0 %all_to_all.15 = bf16[8,256,128]{1,2,0:T(8,128)(2,1)S(1)} all-to-all(bf16[8,256,128]{1,2,0:T(8,128)(2,1)S(1)} %fusion.45), channel_id=1, replica_groups=mesh['kv'=16,'tp'=8] {'tp'}, dimensions={0} | all-to-all | bytes 1048576 | tf_op jit(solution)/shard_map/all_to_all | solution.py:219
  163.3 2.3 %convolution_convert_fusion = bf16[256,2048]{1,0:T(8,128)(2,1)} fusion(bf16[256,1024]{0,1:T(8,128)(2,1)S(1)} %bitcast.199, bf16[1024,2048]{1,0:T(8,128)(2,1)S(1)} %copy-done.20), kind=kOutput, calls=%fused_computation.31 | convolution fusion | flops 1074266112 | bytes 5767168 | tf_op jit(solution)/shard_map/dot_general | solution.py:221
  (111 shorter events, 9.6 us)
Async XLA Ops:
  0.0 29.9 %copy-start = (bf16[1,2048,64]{1,2,0:T(8,128)(2,1)S(1)}, bf16[1,2048,64]{1,2,0:T(8,128)(2,1)}, u32[]{:S(2)}) copy-start(bf16[1,2048,64]{1,2,0:T(8,128)(2,1)} %param.25) | copy-start | bytes 786436
  0.0 5.9 %copy-start.18 = (bf16[1,32,64]{2,1,0:T(8,128)(2,1)S(1)}, bf16[1,32,64]{2,1,0:T(8,128)(2,1)}, u32[]{:S(2)}) copy-start(bf16[1,32,64]{2,1,0:T(8,128)(2,1)} %param.24) | copy-start | bytes 12292
  0.0 6.0 %copy-start.19 = (bf16[1,32,64]{2,1,0:T(8,128)(2,1)S(1)}, bf16[1,32,64]{2,1,0:T(8,128)(2,1)}, u32[]{:S(2)}) copy-start(bf16[1,32,64]{2,1,0:T(8,128)(2,1)} %param.27) | copy-start | bytes 12292
  0.0 7.4 %copy-start.10 = (bf16[2048,64]{0,1:T(8,128)(2,1)S(1)}, bf16[2048,64]{0,1:T(8,128)(2,1)}, u32[]{:S(2)}) copy-start(bf16[2048,64]{0,1:T(8,128)(2,1)} %param.19) | copy-start | bytes 786436
  0.0 8.4 %copy-start.11 = (bf16[2048,64]{0,1:T(8,128)(2,1)S(1)}, bf16[2048,64]{0,1:T(8,128)(2,1)}, u32[]{:S(2)}) copy-start(bf16[2048,64]{0,1:T(8,128)(2,1)} %param.20) | copy-start | bytes 786436
  0.8 8.7 %copy-start.12 = (bf16[2048,64]{0,1:T(8,128)(2,1)S(1)}, bf16[2048,64]{0,1:T(8,128)(2,1)}, u32[]{:S(2)}) copy-start(bf16[2048,64]{0,1:T(8,128)(2,1)} %param.21) | copy-start | bytes 786436
  0.8 9.7 %copy-start.13 = (bf16[2048,64]{0,1:T(8,128)(2,1)S(1)}, bf16[2048,64]{0,1:T(8,128)(2,1)}, u32[]{:S(2)}) copy-start(bf16[2048,64]{0,1:T(8,128)(2,1)} %param.22) | copy-start | bytes 786436
  27.2 1.2 copy-start.9
  27.2 2.7 %copy-start.16 = (bf16[1,64,64]{2,1,0:T(8,128)(2,1)S(1)}, bf16[1,64,64]{2,1,0:T(8,128)(2,1)}, u32[]{:S(2)}) copy-start(bf16[1,64,64]{2,1,0:T(8,128)(2,1)} %param.26) | copy-start | bytes 24580
  27.2 3.0 %copy-start.14 = (bf16[1,2048,64]{1,2,0:T(8,128)(2,1)S(1)}, bf16[1,2048,64]{1,2,0:T(8,128)(2,1)}, u32[]{:S(2)}) copy-start(bf16[1,2048,64]{1,2,0:T(8,128)(2,1)} %param.28) | copy-start | bytes 786436
  27.2 3.0 %copy-start.17 = (bf16[1,64,64]{2,1,0:T(8,128)(2,1)S(1)}, bf16[1,64,64]{2,1,0:T(8,128)(2,1)}, u32[]{:S(2)}) copy-start(bf16[1,64,64]{2,1,0:T(8,128)(2,1)} %param.29) | copy-start | bytes 24580
  27.2 12.8 %copy-start.15 = (s32[1,256,8]{1,2,0:T(8,128)S(1)}, s32[1,256,8]{1,2,0:T(8,128)}, u32[]{:S(2)}) copy-start(s32[1,256,8]{1,2,0:T(8,128)} %param.31) | copy-start | bytes 24580
  31.5 23.7 %all-to-all-start = ((bf16[16,1,64,128]{3,2,1,0:T(8,128)(2,1)}), bf16[16,1,64,128]{3,2,1,0:T(8,128)(2,1)}, u32[]{:S(2)}, u32[]{:S(2)}) async-start(bf16[16,1,64,128]{3,2,1,0:T(8,128)(2,1)} %broadcast_in_dim.34), calls=%async_computation | async-start | bytes 524288 | tf_op jit(solution)/shard_map/all_to_all | solution.py:18
  51.9 3.1 %copy-start.7 = (f32[2048,32]{0,1:T(8,128)S(1)}, f32[2048,32]{0,1:T(8,128)}, u32[]{:S(2)}) copy-start(f32[2048,32]{0,1:T(8,128)} %get-tuple-element.21) | copy-start | bytes 786436
  51.9 3.1 %copy-start.8 = (f32[2048,32]{0,1:T(8,128)S(1)}, f32[2048,32]{0,1:T(8,128)}, u32[]{:S(2)}) copy-start(f32[2048,32]{0,1:T(8,128)} %get-tuple-element.22) | copy-start | bytes 786436
  55.2 9.1 %copy-start.5 = (bf16[8,8,16,128]{3,1,2,0:T(8,128)(2,1)S(1)}, bf16[8,8,16,128]{3,1,2,0:T(8,128)(2,1)}, u32[]{:S(2)}) copy-start(bf16[8,8,16,128]{3,1,2,0:T(8,128)(2,1)} %get-tuple-element.11) | copy-start | bytes 786436
  55.2 67.7 %all-to-all-start.1 = ((bf16[1,16,16,64,128]{4,3,2,0,1:T(8,128)(2,1)}), bf16[1,16,16,64,128]{4,3,2,0,1:T(8,128)(2,1)}, u32[]{:S(2)}, u32[]{:S(2)}) async-start(bf16[1,16,16,64,128]{4,3,2,0,1:T(8,128)(2,1)} %bitcast.184), calls=%async_computation.1 | async-start | bytes 8388608 | tf_op jit(solution)/shard_map/all_to_all | solution.py:181
  130.6 1.6 copy-start.2
  132.1 1.6 copy-start.4
  133.7 7.2 %copy-start.3 = (bf16[1,16,640,128]{2,3,1,0:T(8,128)(2,1)S(1)}, bf16[1,16,640,128]{2,3,1,0:T(8,128)(2,1)}, u32[]{:S(2)}) copy-start(bf16[1,16,640,128]{2,3,1,0:T(8,128)(2,1)} %copy-done.2) | copy-start | bytes 7864324
  140.9 5.9 %copy-start.6 = (f32[2048,2,64]{0,2,1:T(8,128)S(1)}, f32[2048,2,64]{0,2,1:T(8,128)}, u32[]{:S(2)}) copy-start(f32[2048,2,64]{0,2,1:T(8,128)} %fusion.19) | copy-start | bytes 3145732
  146.1 17.2 %copy-start.20 = (bf16[1024,2048]{1,0:T(8,128)(2,1)S(1)}, bf16[1024,2048]{1,0:T(8,128)(2,1)}, u32[]{:S(2)}) copy-start(bf16[1024,2048]{1,0:T(8,128)(2,1)} %param.30) | copy-start | bytes 12582916
  146.7 18.9 %copy-start.1 = (bf16[1,2048,64]{1,2,0:T(8,128)(2,1)S(1)}, bf16[1,2048,64]{1,2,0:T(8,128)(2,1)}, u32[]{:S(2)}) copy-start(bf16[1,2048,64]{1,2,0:T(8,128)(2,1)} %param.25) | copy-start | bytes 786436
